TPU v7x, 32 devices: a whole 2x2x4 slice. The times are simulated.
32 devices in a mesh: kv: 8 (over z, y), tp: 4 (over x, core).
Axes of the slice: x: 2, y: 2, z: 4, core: 2. Of those that a mesh axis runs over, the one named last changes fastest.
Arguments:
- tokens: bfloat16 [16, 4096], P(None, ('kv', 'tp')), may hold values from -8 to 8
- gate_weights: bfloat16 [2, 4096, 11264], P(None, None, ('kv', 'tp')), may hold values from -0.09375 to 0.09375
- up_weights: bfloat16 [2, 4096, 11264], P(None, None, ('kv', 'tp')), may hold values from -0.09375 to 0.09375
- down_weights: bfloat16 [2, 11264, 4096], P(None, ('kv', 'tp')), may hold values from -0.4375 to 0.4375
- norm_gain: bfloat16 [3, 4096], P(None, ('kv', 'tp')), may hold values from 0.25 to 4.5
- norm_bias: bfloat16 [3, 4096], P(None, ('kv', 'tp')), may hold values from -3 to 3
- query_weight: bfloat16 [4096, 4096], P('kv', 'tp'), may hold values from -0.09375 to 0.09375
- forget_weight: bfloat16 [4096, 4096], P('kv', 'tp'), may hold values from -0.09375 to 0.09375
- input_weight: bfloat16 [4096, 4096], P('kv', 'tp'), may hold values from -0.09375 to 0.09375
- outgate_weight: bfloat16 [4096, 4096], P('kv', 'tp'), may hold values from -0.09375 to 0.09375
- lower_bound: float32 [4096], P('tp'), may hold values from 0.05 to 0.9
- head_gain: float32 [4096], P('tp'), may hold values from 0.1 to 1.9
- out_weight: bfloat16 [4096, 4096], P('tp'), may hold values from -0.25 to 0.25
- state: float32 [16, 32, 128, 128], P('kv', 'tp'), may hold values from -3 to 3
Outputs:
- mixed: bfloat16 [16, 4096], P(None, ('kv', 'tp'))
- new_state: float32 [16, 32, 128, 128], P('kv', 'tp')
All inputs are finite; a program needn't handle non-finite values.
Results may differ from a plain program's by a relative error of at most 0.022.
Values may be sent and summed in bfloat16 or wider, within the bound.
A program may use at most 64 MiB of HBM per device.

v0:
```python
import jax
import jax.numpy as jnp
from jax import lax
from jax.sharding import PartitionSpec as P

HEAD = 128


residual_scale = 8.0**0.25
norm_eps = 1e-05
head_eps = 1e-06


def whole_norm(stream, gain_row, bias_row):
    row_mean = jnp.mean(stream, axis=-1, keepdims=True)
    centred = stream - row_mean
    spread = jnp.mean(centred * centred, axis=-1, keepdims=True)
    return centred * lax.rsqrt(spread + norm_eps) * gain_row.astype(jnp.float32) + bias_row.astype(
        jnp.float32
    )


def ffn_partial(whole_rows, gate_w, up_w, down_w):
    gate_proj = jnp.dot(whole_rows, gate_w, preferred_element_type=jnp.float32)
    up_proj = jnp.dot(whole_rows, up_w, preferred_element_type=jnp.float32)
    hidden = (jax.nn.silu(gate_proj) * up_proj).astype(jnp.bfloat16)
    return jnp.dot(hidden, down_w, preferred_element_type=jnp.float32)


def local(
    tokens,
    gate_weights,
    up_weights,
    down_weights,
    norm_gain,
    norm_bias,
    query_weight,
    forget_weight,
    input_weight,
    outgate_weight,
    lower_bound,
    head_gain,
    out_weight,
    state,
):
    own_cols = tokens.shape[1]
    col_offset = lax.axis_index(("kv", "tp")) * own_cols
    whole_tokens, whole_gain, whole_bias = (
        lax.all_gather(tokens, ("kv", "tp"), axis=1, tiled=True),
        lax.all_gather(norm_gain, ("kv", "tp"), axis=1, tiled=True),
        lax.all_gather(norm_bias, ("kv", "tp"), axis=1, tiled=True),
    )

    def finish(partial_value, residual_whole, index, want_whole):
        total = lax.psum(partial_value, ("kv", "tp"))
        stream = residual_scale * residual_whole + 0.5 * total
        normed = whole_norm(stream, whole_gain[index], whole_bias[index]).astype(jnp.bfloat16)
        if want_whole:
            return normed
        return lax.dynamic_slice_in_dim(normed, col_offset, own_cols, 1)

    partial_one = ffn_partial(whole_tokens, gate_weights[0], up_weights[0], down_weights[0])
    normed_one = finish(partial_one, whole_tokens.astype(jnp.float32), 0, True)
    seq_count = state.shape[0]
    head_count = state.shape[1]
    head_cols = query_weight.shape[1]
    weight_rows = query_weight.shape[0]
    seq_offset = lax.axis_index("kv") * seq_count
    block_rows = lax.dynamic_slice_in_dim(
        normed_one, lax.axis_index("kv") * weight_rows, weight_rows, 1
    )
    weights = (query_weight, forget_weight, input_weight, outgate_weight)
    projected = lax.psum_scatter(
        jnp.concatenate(
            [jnp.dot(block_rows, weight, preferred_element_type=jnp.float32) for weight in weights],
            axis=1,
        ).astype(jnp.bfloat16),
        "kv",
        scatter_dimension=0,
        tiled=True,
    )
    query_pre = projected[:, :head_cols].astype(jnp.float32).reshape(seq_count, head_count, HEAD)
    forget_pre = (
        projected[:, head_cols : 2 * head_cols]
        .astype(jnp.float32)
        .reshape(seq_count, head_count, HEAD)
    )
    input_pre = (
        projected[:, 2 * head_cols : 3 * head_cols]
        .astype(jnp.float32)
        .reshape(seq_count, head_count, HEAD)
    )
    outgate_pre = projected[:, 3 * head_cols :].astype(jnp.float32)
    low_bound = lower_bound.reshape(head_count, HEAD)
    forget = low_bound + (1.0 - low_bound) * jax.nn.sigmoid(forget_pre)
    key_part = (1.0 - low_bound) * jax.nn.sigmoid(-forget_pre)
    updated = forget[..., None] * state + key_part[..., None] * input_pre[:, :, None, :]
    readout = jnp.einsum(
        "shd,shde->she", jax.nn.silu(query_pre), updated, precision=lax.Precision.HIGHEST
    )
    readout = readout * lax.rsqrt(jnp.mean(readout * readout, axis=-1, keepdims=True) + head_eps)
    gated_out = (
        readout.reshape(seq_count, head_cols) * head_gain * jax.nn.silu(outgate_pre)
    ).astype(jnp.bfloat16)
    mixer_part = jnp.dot(gated_out, out_weight, preferred_element_type=jnp.float32)
    head_sum = lax.psum_scatter(
        mixer_part.astype(jnp.bfloat16), "tp", scatter_dimension=1, tiled=True
    ).astype(jnp.float32)
    piece_cols = head_sum.shape[1]
    own_normed = lax.dynamic_slice_in_dim(normed_one, seq_offset, seq_count, 0)
    own_normed = lax.dynamic_slice_in_dim(
        own_normed, lax.axis_index("tp") * piece_cols, piece_cols, 1
    )
    stream_own = (residual_scale * own_normed.astype(jnp.float32) + head_sum).astype(jnp.bfloat16)
    seq_rows = lax.all_gather(stream_own, "tp", axis=1, tiled=True)
    stream_two = lax.all_gather(seq_rows, "kv", axis=0, tiled=True)
    normed_two = whole_norm(stream_two.astype(jnp.float32), whole_gain[1], whole_bias[1]).astype(
        jnp.bfloat16
    )
    partial_two = ffn_partial(normed_two, gate_weights[1], up_weights[1], down_weights[1])
    mixed = finish(partial_two, normed_two.astype(jnp.float32), 2, False)
    return (mixed, updated)


def solution(mesh):
    return jax.shard_map(
        local,
        mesh=mesh,
        in_specs=(
            P(None, ("kv", "tp")),
            P(None, None, ("kv", "tp")),
            P(None, None, ("kv", "tp")),
            P(None, ("kv", "tp"), None),
            P(None, ("kv", "tp")),
            P(None, ("kv", "tp")),
            P("kv", "tp"),
            P("kv", "tp"),
            P("kv", "tp"),
            P("kv", "tp"),
            P("tp"),
            P("tp"),
            P("tp", None),
            P("kv", "tp", None, None),
        ),
        out_specs=(P(None, ("kv", "tp")), P("kv", "tp", None, None)),
        check_vma=False,
    )
```

profile of v0, /device:TPU:0, one launch (start us, length us, event | category | flops | bytes accessed | tf_op | source)
XLA Modules:
  0.0 475.1 jit_solution(1916518418078540519)
XLA Ops:
  7.3 44.0 %all_gather.15 = bf16[16,4096]{1,0:T(8,128)(2,1)S(1)} all-gather(bf16[16,128]{1,0:T(8,128)(2,1)} %param.14), channel_id=1, replica_groups=mesh['kv'=8,'tp'=4] {'kv','tp'}, dimensions={1}, use_global_device_ids=true | all-gather | bytes 135168 | tf_op jit(solution)/shard_map/all_gather | solution.py:49
  51.2 2.7 fusion.10
  54.0 5.5 %fusion.6 = f32[16,4096]{1,0:T(8,128)} fusion(bf16[2,352,4096]{2,1,0:T(8,128)(2,1)} %param.17, bf16[16,4096]{1,0:T(8,128)(2,1)S(1)} %all_gather.15, bf16[2,4096,352]{1,2,0:T(8,128)(2,1)} %param.16, f32[16,352]{1,0:T(8,128)S(1)} %fusion.10), kind=kOutput, calls=%fused_computation.7 | convolution fusion | flops 92308480 | bytes 6182912 | tf_op jit(solution)/shard_map/dot_general | solution.py:27
  59.6 36.7 %all_gather.16 = bf16[3,4096]{1,0:T(4,128)(2,1)S(1)} all-gather(bf16[3,128]{1,0:T(4,128)(2,1)S(1)} %copy-done.6), channel_id=1, replica_groups=mesh['kv'=8,'tp'=4] {'kv','tp'}, dimensions={1}, use_global_device_ids=true | all-gather | bytes 25344 | tf_op jit(solution)/shard_map/all_gather | solution.py:50
  96.3 38.1 %all_gather.17 = bf16[3,4096]{1,0:T(4,128)(2,1)S(1)} all-gather(bf16[3,128]{1,0:T(4,128)(2,1)S(1)} %copy-done.7), channel_id=1, replica_groups=mesh['kv'=8,'tp'=4] {'kv','tp'}, dimensions={1}, use_global_device_ids=true | all-gather | bytes 25344 | tf_op jit(solution)/shard_map/all_gather | solution.py:51
  134.5 0.6 dynamic-slice
  135.7 46.7 %all-reduce.5.cloned.1.call-done = f32[16,4096]{1,0:T(8,128)} async-done(((f32[16,4096]{1,0:T(8,128)}), f32[16,4096]{1,0:T(8,128)}) %all-reduce.5.cloned.1.call-update) | async-done | bytes 262160 | tf_op jit(solution)/shard_map/psum | solution.py:55
  182.4 1.1 fusion.36
  183.5 1.2 multiply_reduce_fusion.2
  184.7 1.1 add_convert_fusion.1
  185.8 0.2 convolution_convert_fusion.3
  186.0 0.3 convolution_convert_fusion.2
  186.3 0.3 convolution_convert_fusion.1
  186.5 1.5 convolution_convert_fusion.4
  188.0 0.7 pad_maximum_fusion
  188.8 69.5 %all-reduce.9.cloned.1.call-done = bf16[16,4096]{1,0:T(8,128)(2,1)} async-done(((bf16[16,4096]{1,0:T(8,128)(2,1)}), bf16[16,4096]{1,0:T(8,128)(2,1)}) %all-reduce.9.cloned.1.call-update) | async-done | bytes 131088
  258.3 0.8 convert_bitcast_fusion
  259.1 0.8 fusion.57
  260.0 1.8 multiply_add_fusion
  261.8 1.0 fusion.83
  263.0 4.7 convolution_convert_fusion
  267.6 1.4 copy.18
  269.2 24.0 %reduce-scatter.4.cloned.1.call-done = bf16[1024,2]{1,0:T(8,128)(2,1)} async-done(((bf16[4096,2]{1,0:T(8,128)(2,1)}), bf16[1024,2]{1,0:T(8,128)(2,1)}) %reduce-scatter.4.cloned.1.call-update) | async-done | bytes 4112
  293.1 1.1 copy.19
  294.3 5.2 %all_gather.18 = bf16[2,4096]{1,0:T(2,128)(2,1)S(1)} all-gather(bf16[2,1024]{1,0:T(2,128)(2,1)S(1)} %add_convert_fusion.2), channel_id=1, replica_groups=mesh['kv'=8,'tp'=4] {'tp'}, dimensions={1}, use_global_device_ids=true | all-gather | bytes 20480 | tf_op jit(solution)/shard_map/all_gather | solution.py:115
  299.5 30.6 %all-gather = bf16[8,2,4096]{2,1,0:T(2,128)(2,1)S(1)} all-gather(bf16[1,2,4096]{2,1,0:T(2,128)(2,1)S(1)} %bitcast.107), channel_id=1, replica_groups=mesh['kv'=8,'tp'=4] {'kv'}, dimensions={0}, use_global_device_ids=true | all-gather | bytes 147456 | tf_op jit(solution)/shard_map/all_gather | solution.py:116
  330.6 2.7 fusion.4
  333.3 5.4 %fusion = f32[16,4096]{1,0:T(8,128)} fusion(bf16[2,352,4096]{2,1,0:T(8,128)(2,1)} %param.17, bf16[2,4096,352]{1,2,0:T(8,128)(2,1)} %param.16, f32[16,352]{1,0:T(8,128)S(1)} %fusion.4, f32[16,4096]{1,0:T(8,128)S(1)} %reshape.110, f32[4096]{0:T(1024)S(1)} %bitcast.101, f32[4096]{0:T(1024)S(1)} %bitcast.97, f32[16]{0:T(128)S(1)} %add_rsqrt_fusion.2, ...), kind=kOutput, calls=%fused_computation.1 | convolution fusion | flops 92636160 | bytes 6346880 | tf_op jit(solution)/shard_map/dot_general | solution.py:27
  338.9 126.6 %all-reduce.7.cloned.1.call-done = f32[16,4096]{1,0:T(8,128)} async-done(((f32[16,4096]{1,0:T(8,128)}), f32[16,4096]{1,0:T(8,128)}) %all-reduce.7.cloned.1.call-update) | async-done | bytes 262160 | tf_op jit(solution)/shard_map/psum | solution.py:55
  465.5 1.2 fusion.35
  466.7 1.2 multiply_reduce_fusion
  467.9 0.7 fusion.69
  (48 shorter events, 1.4 us)
Async XLA Ops:
  7.2 178.6 %copy-start = (bf16[512,1024]{1,0:T(8,128)(2,1)S(1)}, bf16[512,1024]{1,0:T(8,128)(2,1)}, u32[]{:S(2)}) copy-start(bf16[512,1024]{1,0:T(8,128)(2,1)} %param.21) | copy-start | bytes 3145732
  7.2 127.3 %copy-start.8 = (u32[32]{0:T(128)S(1)}, u32[32]{0:T(128)}, u32[]{:S(2)}) copy-start(u32[32]{0:T(128)} %constant.72) | copy-start | bytes 388
  7.2 52.4 %copy-start.6 = (bf16[3,128]{1,0:T(4,128)(2,1)S(1)}, bf16[3,128]{1,0:T(4,128)(2,1)}, u32[]{:S(2)}) copy-start(bf16[3,128]{1,0:T(4,128)(2,1)} %param.18) | copy-start | bytes 2308
  7.2 89.1 %copy-start.7 = (bf16[3,128]{1,0:T(4,128)(2,1)S(1)}, bf16[3,128]{1,0:T(4,128)(2,1)}, u32[]{:S(2)}) copy-start(bf16[3,128]{1,0:T(4,128)(2,1)} %param.19) | copy-start | bytes 2308
  7.2 175.2 %all-reduce.5.cloned.1.call-start = ((), (), s32[]{:S(2)}) async-start(), calls=%async_computation.1 | async-start | bytes 524288 | tf_op jit(solution)/shard_map/psum | solution.py:55
  51.2 134.8 %copy-start.2 = (bf16[512,1024]{1,0:T(8,128)(2,1)S(1)}, bf16[512,1024]{1,0:T(8,128)(2,1)}, u32[]{:S(2)}) copy-start(bf16[512,1024]{1,0:T(8,128)(2,1)} %param.22) | copy-start | bytes 3145732
  54.0 132.3 %copy-start.3 = (bf16[512,1024]{1,0:T(8,128)(2,1)S(1)}, bf16[512,1024]{1,0:T(8,128)(2,1)}, u32[]{:S(2)}) copy-start(bf16[512,1024]{1,0:T(8,128)(2,1)} %param.23) | copy-start | bytes 3145732
  54.0 134.8 %copy-start.5 = (f32[1024]{0:T(1024)S(1)}, f32[1024]{0:T(1024)}, u32[]{:S(2)}) copy-start(f32[1024]{0:T(1024)} %param.24) | copy-start | bytes 12292
  59.5 203.5 %copy-start.4 = (f32[1024]{0:T(1024)S(1)}, f32[1024]{0:T(1024)}, u32[]{:S(2)}) copy-start(f32[1024]{0:T(1024)} %param.25) | copy-start | bytes 12292
  59.5 198.8 %all-reduce.9.cloned.1.call-start = ((), (), s32[]{:S(2)}) async-start(), calls=%async_computation.4 | async-start | bytes 262144
  188.7 104.4 %reduce-scatter.4.cloned.1.call-start = ((), (), s32[]{:S(2)}) async-start(), calls=%async_computation.3 | async-start | bytes 1310720
  261.8 5.8 %copy-start.1 = (f32[2,8,128,128]{3,2,1,0:T(8,128)}, f32[2,8,128,128]{3,2,1,0:T(8,128)S(1)}, u32[]{:S(2)}) copy-start(f32[2,8,128,128]{3,2,1,0:T(8,128)S(1)} %multiply_add_fusion) | copy-start | bytes 3145732
  269.1 196.4 %all-reduce.7.cloned.1.call-start = ((), (), s32[]{:S(2)}) async-start(), calls=%async_computation.2 | async-start | bytes 524288 | tf_op jit(solution)/shard_map/psum | solution.py:55
Sparse Core Ops, SparseCore 0:
  59.6 122.7 all-reduce.4
  188.8 69.4 all-reduce.8
  269.2 23.8 reduce-scatter.3
  338.9 126.5 all-reduce.6
where the time goes:
time: 476 us; the launch traced here: 475 us
  waiting for transfers between devices  267 us (56%)
  blocking collectives  155 us (33%)
  matrix products  24.2 us (5%)
  between operations  14.6 us (3%)
  other arithmetic  11.4 us (2%)
    psum x2, waiting for transfers between devices, finish(): total = lax.psum(partial_value, ('kv', 'tp'))  173 us
    unnamed x6, waiting for transfers between devices  93.6 us
    all_gather x1, blocking collectives, local(): lax.all_gather(tokens, ('kv', 'tp'), axis=1, tiled=True)  44 us
    all_gather x1, blocking collectives, local(): lax.all_gather(norm_bias, ('kv', 'tp'), axis=1, tiled=True)  38.1 us
    all_gather x1, blocking collectives, local(): lax.all_gather(norm_gain, ('kv', 'tp'), axis=1, tiled=True)  36.7 us
    all_gather x1, blocking collectives, local(): stream_two = lax.all_gather(seq_rows, 'kv', axis=0, tiled=True)  30.6 us
    dot_general x2, matrix products, ffn_partial(): return jnp.dot(hidden, down_w, preferred_element_type=jnp.float32)  10.9 us
  transfers between devices with their start and end apart: 4, of which 4 were waited for; matrix products, arithmetic and copies ran while one was open for 0% of the time, Pallas kernels for 0%

commit v1 on v0

--- a/solution.py
+++ b/solution.py
@@ -1,7 +1,13 @@
+import functools
+
 import jax
 import jax.numpy as jnp
 from jax import lax
+from jax.experimental import pallas as pl
+from jax.experimental.pallas import tpu as pltpu
 from jax.sharding import PartitionSpec as P
+
+MESH = pl.DeviceIdType.MESH
 
 HEAD = 128
 
@@ -122,9 +128,440 @@
     return (mixed, updated)
 
 
+TOK, GB, RS_ONE, AG_ONE, RS_KV, RS_TP, AG_TWO, RS_THREE, AG_THREE = range(9)
+PHASES = 9
+
+
+def tree_sum(terms):
+    while len(terms) > 1:
+        rest = [terms[-1]] if len(terms) % 2 else []
+        terms = [a + b for a, b in zip(terms[::2], terms[1::2])] + rest
+    return terms[0]
+
+
+def layer_kernel(
+    n_kv,
+    n_tp,
+    tokens_ref,
+    gain_ref,
+    bias_ref,
+    low_ref,
+    head_gain_ref,
+    gate_hbm,
+    up_hbm,
+    down_hbm,
+    query_hbm,
+    forget_hbm,
+    input_hbm,
+    outgate_hbm,
+    out_hbm,
+    state_hbm,
+    mixed_ref,
+    state_out,
+    gate_v,
+    up_v,
+    down_v,
+    proj_v,
+    out_v,
+    state_v,
+    new_v,
+    tok_buf,
+    gb_own,
+    gb_buf,
+    rs_send,
+    rs_recv_one,
+    rs_recv_three,
+    own_ag,
+    ag_one,
+    normed_f32,
+    normed_bf,
+    proj_f32,
+    proj_send,
+    proj_recv,
+    gated_buf,
+    tp_f32,
+    tp_send,
+    tp_recv,
+    own_ag_two,
+    ag_two,
+    ag_two_f32,
+    own_ag_three,
+    ag_three,
+    final_buf,
+    send_sem,
+    recv_sem,
+    load_sem,
+    store_sem,
+):
+    n = n_kv * n_tp
+    batch, lane = tokens_ref.shape
+    width = n * lane
+    seqs, heads = state_v.shape[0], state_v.shape[1]
+    kv, tp = lax.axis_index("kv"), lax.axis_index("tp")
+    me = kv * n_tp + tp
+
+    proj_hbm = (query_hbm, forget_hbm, input_hbm, outgate_hbm)
+    loads = {}
+    order = [("gate0", gate_hbm.at[0], gate_v.at[0]), ("up0", up_hbm.at[0], up_v.at[0])]
+    order += [("down0", down_hbm.at[0], down_v.at[0])]
+    order += [("proj%d" % i, proj_hbm[i], proj_v.at[i]) for i in range(4)]
+    order += [("state", state_hbm, state_v), ("out", out_hbm, out_v)]
+    order += [("gate1", gate_hbm.at[1], gate_v.at[1]), ("up1", up_hbm.at[1], up_v.at[1])]
+    order += [("down1", down_hbm.at[1], down_v.at[1])]
+    for i, (name, source, target) in enumerate(order):
+        loads[name] = pltpu.make_async_copy(source, target, load_sem.at[i])
+        loads[name].start()
+
+    def peer_id(k):
+        peer = lax.rem(me + k, n)
+        return peer, (lax.div(peer, n_tp), lax.rem(peer, n_tp))
+
+    barrier = pltpu.get_barrier_semaphore()
+
+    @pl.loop(1, n)
+    def _(k):
+        _, device = peer_id(k)
+        pl.semaphore_signal(barrier, inc=1, device_id=device, device_id_type=MESH)
+
+    def slot(ref, index, rows):
+        return ref.at[pl.ds(pl.multiple_of(index * rows, rows), rows)]
+
+    def send_all(phase, src_of, dst, count, device_of):
+        @pl.loop(1, count)
+        def _(k):
+            index, device = device_of(k)
+            pltpu.make_async_remote_copy(
+                src_ref=src_of(index),
+                dst_ref=dst,
+                send_sem=send_sem.at[phase],
+                recv_sem=recv_sem.at[phase],
+                device_id=device,
+                device_id_type=MESH,
+            ).start()
+
+    def wait_bytes(sem, ref, rows):
+        part = ref.at[pl.ds(0, rows)]
+        pltpu.make_async_copy(part, part, sem).wait()
+
+    gb_own[...] = jnp.zeros(gb_own.shape, jnp.float32)
+    gb_own[0:3, :] = gain_ref[...].astype(jnp.float32)
+    gb_own[3:6, :] = bias_ref[...].astype(jnp.float32)
+    slot(gb_buf, me, 8)[...] = gb_own[...]
+    slot(tok_buf, me, batch)[...] = tokens_ref[...]
+
+    pl.semaphore_wait(barrier, n - 1)
+    send_all(TOK, lambda i: tokens_ref, slot(tok_buf, me, batch), n, peer_id)
+    send_all(GB, lambda i: gb_own, slot(gb_buf, me, 8), n, peer_id)
+
+    def tiles_of(ref):
+        return [ref[j * batch : (j + 1) * batch, :].astype(jnp.float32) for j in range(n)]
+
+    def stats(tiles):
+        mean = jnp.sum(tree_sum(tiles), axis=1, keepdims=True) / width
+        centred = [tile - mean for tile in tiles]
+        spread = jnp.sum(tree_sum([c * c for c in centred]), axis=1, keepdims=True) / width
+        return mean, centred, lax.rsqrt(spread + norm_eps)
+
+    def norm_tiles(tiles, index):
+        _, centred, scale = stats(tiles)
+        return [
+            c * scale * gb_buf[8 * j + index : 8 * j + index + 1, :]
+            + gb_buf[8 * j + 3 + index : 8 * j + 4 + index, :]
+            for j, c in enumerate(centred)
+        ]
+
+    def ffn(rows, layer):
+        step = 4 * lane
+        gate = jnp.zeros((batch, gate_v.shape[2]), jnp.float32)
+        up = jnp.zeros((batch, gate_v.shape[2]), jnp.float32)
+        loads["gate%d" % layer].wait()
+        loads["up%d" % layer].wait()
+        for k in range(0, width, step):
+            piece = rows[:, k : k + step]
+            gate += jnp.dot(
+                piece, gate_v[layer, k : k + step, :], preferred_element_type=jnp.float32
+            )
+            up += jnp.dot(piece, up_v[layer, k : k + step, :], preferred_element_type=jnp.float32)
+        hidden = (jax.nn.silu(gate) * up).astype(jnp.bfloat16)
+        loads["down%d" % layer].wait()
+        for k in range(0, width, step):
+            part = jnp.dot(
+                hidden, down_v[layer, :, k : k + step], preferred_element_type=jnp.float32
+            ).astype(jnp.bfloat16)
+            for j in range(step // lane):
+                first = (k // lane + j) * batch
+                rs_send[first : first + batch, :] = part[:, j * lane : (j + 1) * lane]
+
+    def reduce_scatter(phase, recv):
+        send_all(phase, lambda i: slot(rs_send, i, batch), slot(recv, me, batch), n, peer_id)
+        slot(recv, me, batch)[...] = slot(rs_send, me, batch)[...]
+        wait_bytes(recv_sem.at[phase], recv, (n - 1) * batch)
+        return tree_sum(tiles_of(recv))
+
+    wait_bytes(recv_sem.at[TOK], tok_buf, (n - 1) * batch)
+    ffn(jnp.concatenate([tok_buf[j * batch : (j + 1) * batch, :] for j in range(n)], axis=1), 0)
+    total = reduce_scatter(RS_ONE, rs_recv_one)
+    stream = residual_scale * tokens_ref[...].astype(jnp.float32) + 0.5 * total
+    own_ag[...] = stream.astype(jnp.bfloat16)
+    slot(ag_one, me, batch)[...] = stream.astype(jnp.bfloat16)
+    send_all(AG_ONE, lambda i: own_ag, slot(ag_one, me, batch), n, peer_id)
+    wait_bytes(recv_sem.at[GB], gb_buf, (n - 1) * 8)
+    wait_bytes(recv_sem.at[AG_ONE], ag_one, (n - 1) * batch)
+    for j, tile in enumerate(norm_tiles(tiles_of(ag_one), 0)):
+        rounded = tile.astype(jnp.bfloat16)
+        normed_bf[j * batch : (j + 1) * batch, :] = rounded
+        normed_f32[j * batch : (j + 1) * batch, :] = rounded.astype(jnp.float32)
+
+    own_rows = slot(normed_bf, kv, n_tp * batch)
+    block = jnp.concatenate(
+        [own_rows[j * batch : (j + 1) * batch, :] for j in range(n_tp)], axis=1
+    )
+    per_seq = 4 * heads
+    for i in range(4):
+        loads["proj%d" % i].wait()
+        part = jnp.dot(block, proj_v[i], preferred_element_type=jnp.float32)
+        for h in range(heads):
+            for r in range(0, batch, 8):
+                proj_f32[pl.ds(r * per_seq + i * heads + h, 8, stride=per_seq), :] = part[
+                    r : r + 8, h * HEAD : (h + 1) * HEAD
+                ]
+    proj_send[...] = proj_f32[...].astype(jnp.bfloat16)
+    block_len = seqs * per_seq
+
+    def kv_peer(k):
+        peer = lax.rem(kv + k, n_kv)
+        return peer, (peer, tp)
+
+    send_all(
+        RS_KV,
+        lambda i: slot(proj_send, i, block_len),
+        slot(proj_recv, kv, block_len),
+        n_kv,
+        kv_peer,
+    )
+    slot(proj_recv, kv, block_len)[...] = slot(proj_send, kv, block_len)[...]
+    wait_bytes(recv_sem.at[RS_KV], proj_recv, (n_kv - 1) * block_len)
+    projected = tree_sum(
+        [
+            proj_recv[j * block_len : (j + 1) * block_len, :].astype(jnp.float32)
+            for j in range(n_kv)
+        ]
+    )
+    projected = projected.astype(jnp.bfloat16).astype(jnp.float32)
+
+    low = low_ref[...]
+    loads["state"].wait()
+    for s in range(seqs):
+        base = s * per_seq
+        query_pre = projected[base : base + heads]
+        forget_pre = projected[base + heads : base + 2 * heads]
+        input_pre = projected[base + 2 * heads : base + 3 * heads]
+        outgate_pre = projected[base + 3 * heads : base + 4 * heads]
+        forget = low + (1.0 - low) * jax.nn.sigmoid(forget_pre)
+        key_part = (1.0 - low) * jax.nn.sigmoid(-forget_pre)
+        fill = jnp.zeros((HEAD - 3 * heads, HEAD), jnp.float32)
+        turned = jnp.concatenate([forget, key_part, jax.nn.silu(query_pre), fill], axis=0).T
+        readouts = []
+        for h in range(heads):
+            updated = (
+                turned[:, h : h + 1] * state_v[s, h]
+                + turned[:, heads + h : heads + h + 1] * input_pre[h : h + 1, :]
+            )
+            new_v[s, h] = updated
+            query_col = turned[:, 2 * heads + h : 2 * heads + h + 1]
+            readouts.append(jnp.sum(query_col * updated, axis=0, keepdims=True))
+        readout = jnp.concatenate(readouts, axis=0)
+        mean_square = jnp.mean(readout * readout, axis=1, keepdims=True)
+        readout = readout * lax.rsqrt(mean_square + head_eps)
+        gated_buf[s * heads : (s + 1) * heads, :] = (
+            readout * head_gain_ref[...] * jax.nn.silu(outgate_pre)
+        )
+    store = pltpu.make_async_copy(new_v, state_out, store_sem)
+    store.start()
+
+    gated = jnp.concatenate(
+        [gated_buf[pl.ds(h, seqs, stride=heads), :] for h in range(heads)], axis=1
+    ).astype(jnp.bfloat16)
+    loads["out"].wait()
+    step = 4 * lane
+    rows_tp = seqs * heads
+    for k in range(0, width, step):
+        part = jnp.dot(gated, out_v[:, k : k + step], preferred_element_type=jnp.float32)
+        for j in range(step // lane):
+            tile = k // lane + j
+            first = (tile // heads) * rows_tp + tile % heads
+            tp_f32[pl.ds(first, seqs, stride=heads), :] = part[:, j * lane : (j + 1) * lane]
+    tp_send[...] = tp_f32[...].astype(jnp.bfloat16)
+
+    def tp_peer(k):
+        peer = lax.rem(tp + k, n_tp)
+        return peer, (kv, peer)
+
+    send_all(
+        RS_TP, lambda i: slot(tp_send, i, rows_tp), slot(tp_recv, tp, rows_tp), n_tp, tp_peer
+    )
+    slot(tp_recv, tp, rows_tp)[...] = slot(tp_send, tp, rows_tp)[...]
+    residual = jnp.concatenate(
+        [
+            normed_f32[pl.ds(tp * (heads * batch) + kv * seqs + s, heads, stride=batch), :]
+            for s in range(seqs)
+        ],
+        axis=0,
+    )
+    wait_bytes(recv_sem.at[RS_TP], tp_recv, (n_tp - 1) * rows_tp)
+    head_sum = tree_sum(
+        [tp_recv[j * rows_tp : (j + 1) * rows_tp, :].astype(jnp.float32) for j in range(n_tp)]
+    )
+    stream_two = (residual_scale * residual + head_sum).astype(jnp.bfloat16)
+    own_ag_two[...] = stream_two
+    slot(ag_two, me, rows_tp)[...] = stream_two
+    send_all(AG_TWO, lambda i: own_ag_two, slot(ag_two, me, rows_tp), n, peer_id)
+    wait_bytes(recv_sem.at[AG_TWO], ag_two, (n - 1) * rows_tp)
+    ag_two_f32[...] = ag_two[...].astype(jnp.float32)
+    tiles = [
+        jnp.concatenate(
+            [
+                ag_two_f32[
+                    pl.ds((j // heads) * rows_tp + s * heads + j % heads, n_kv, stride=n_tp * rows_tp),
+                    :,
+                ]
+                for s in range(seqs)
+            ],
+            axis=0,
+        )
+        for j in range(n)
+    ]
+    normed = [tile.astype(jnp.bfloat16) for tile in norm_tiles(tiles, 1)]
+    wait_bytes(send_sem.at[RS_ONE], rs_recv_one, (n - 1) * batch)
+    for j, tile in enumerate(normed):
+        normed_bf[j * batch : (j + 1) * batch, :] = tile
+    ffn(jnp.concatenate(normed, axis=1), 1)
+    total = reduce_scatter(RS_THREE, rs_recv_three)
+    residual = slot(normed_bf, me, batch)[...].astype(jnp.float32)
+    stream = residual_scale * residual + 0.5 * total
+    own_ag_three[...] = stream.astype(jnp.bfloat16)
+    slot(ag_three, me, batch)[...] = stream.astype(jnp.bfloat16)
+    send_all(AG_THREE, lambda i: own_ag_three, slot(ag_three, me, batch), n, peer_id)
+    wait_bytes(recv_sem.at[AG_THREE], ag_three, (n - 1) * batch)
+    mean, _, scale = stats(tiles_of(ag_three))
+    mixed = (stream - mean) * scale * gb_own[2:3, :] + gb_own[5:6, :]
+    for s in range(seqs):
+        final_buf[pl.ds(s, n_kv, stride=seqs), :] = mixed[s * n_kv : (s + 1) * n_kv, :]
+    mixed_ref[...] = final_buf[...].astype(jnp.bfloat16)
+
+    for phase in (TOK, AG_ONE, AG_TWO, RS_THREE, AG_THREE):
+        wait_bytes(send_sem.at[phase], tok_buf, (n - 1) * batch)
+    wait_bytes(send_sem.at[GB], gb_buf, (n - 1) * 8)
+    wait_bytes(send_sem.at[RS_KV], proj_recv, (n_kv - 1) * block_len)
+    wait_bytes(send_sem.at[RS_TP], tp_recv, (n_tp - 1) * rows_tp)
+    store.wait()
+
+
+def fused(n_kv, n_tp, *args):
+    (
+        tokens,
+        gate_weights,
+        up_weights,
+        down_weights,
+        norm_gain,
+        norm_bias,
+        query_weight,
+        forget_weight,
+        input_weight,
+        outgate_weight,
+        lower_bound,
+        head_gain,
+        out_weight,
+        state,
+    ) = args
+    batch, lane = tokens.shape
+    n = n_kv * n_tp
+    seqs, heads = state.shape[:2]
+    bf16, f32 = jnp.bfloat16, jnp.float32
+    per_seq = 4 * heads
+    rows_tp = seqs * heads
+    scratch = [
+        pltpu.VMEM(gate_weights.shape, bf16),
+        pltpu.VMEM(up_weights.shape, bf16),
+        pltpu.VMEM(down_weights.shape, bf16),
+        pltpu.VMEM((4, *query_weight.shape), bf16),
+        pltpu.VMEM(out_weight.shape, bf16),
+        pltpu.VMEM(state.shape, f32),
+        pltpu.VMEM(state.shape, f32),
+        pltpu.VMEM((n * batch, lane), bf16),
+        pltpu.VMEM((8, lane), f32),
+        pltpu.VMEM((n * 8, lane), f32),
+        pltpu.VMEM((n * batch, lane), bf16),
+        pltpu.VMEM((n * batch, lane), bf16),
+        pltpu.VMEM((n * batch, lane), bf16),
+        pltpu.VMEM((batch, lane), bf16),
+        pltpu.VMEM((n * batch, lane), bf16),
+        pltpu.VMEM((n * batch, lane), f32),
+        pltpu.VMEM((n * batch, lane), bf16),
+        pltpu.VMEM((batch * per_seq, HEAD), f32),
+        pltpu.VMEM((batch * per_seq, HEAD), bf16),
+        pltpu.VMEM((batch * per_seq, HEAD), bf16),
+        pltpu.VMEM((rows_tp, HEAD), f32),
+        pltpu.VMEM((n_tp * rows_tp, HEAD), f32),
+        pltpu.VMEM((n_tp * rows_tp, HEAD), bf16),
+        pltpu.VMEM((n_tp * rows_tp, HEAD), bf16),
+        pltpu.VMEM((rows_tp, HEAD), bf16),
+        pltpu.VMEM((n * rows_tp, HEAD), bf16),
+        pltpu.VMEM((n * rows_tp, HEAD), f32),
+        pltpu.VMEM((batch, lane), bf16),
+        pltpu.VMEM((n * batch, lane), bf16),
+        pltpu.VMEM((batch, lane), f32),
+        pltpu.SemaphoreType.DMA((PHASES,)),
+        pltpu.SemaphoreType.DMA((PHASES,)),
+        pltpu.SemaphoreType.DMA((12,)),
+        pltpu.SemaphoreType.DMA,
+    ]
+    vmem = pl.BlockSpec(memory_space=pltpu.VMEM)
+    hbm = pl.BlockSpec(memory_space=pl.ANY)
+    return pl.pallas_call(
+        functools.partial(layer_kernel, n_kv, n_tp),
+        out_shape=(
+            jax.ShapeDtypeStruct(tokens.shape, bf16),
+            jax.ShapeDtypeStruct(state.shape, f32),
+        ),
+        in_specs=[vmem] * 5 + [hbm] * 9,
+        out_specs=(vmem, hbm),
+        scratch_shapes=scratch,
+        compiler_params=pltpu.CompilerParams(
+            collective_id=0, has_side_effects=True, vmem_limit_bytes=60 * 1024 * 1024
+        ),
+        name="layer",
+    )(
+        tokens,
+        norm_gain,
+        norm_bias,
+        lower_bound.reshape(heads, HEAD),
+        head_gain.reshape(heads, HEAD),
+        gate_weights,
+        up_weights,
+        down_weights,
+        query_weight,
+        forget_weight,
+        input_weight,
+        outgate_weight,
+        out_weight,
+        state,
+    )
+
+
+def dispatch(n_kv, n_tp, *args):
+    tokens, state = args[0], args[13]
+    batch, lane = tokens.shape
+    whole_tiles = lane == HEAD and batch % 16 == 0 and (state.shape[0] * state.shape[1]) % 16 == 0
+    if whole_tiles and state.shape[1] == 8 and n_kv % 8 == 0:
+        return fused(n_kv, n_tp, *args)
+    return local(*args)
+
+
 def solution(mesh):
+    n_kv, n_tp = mesh.shape["kv"], mesh.shape["tp"]
     return jax.shard_map(
-        local,
+        functools.partial(dispatch, n_kv, n_tp),
         mesh=mesh,
         in_specs=(
             P(None, ("kv", "tp")),

time: 476 us -> 78 us (0.16)
  waiting for transfers between devices: 267 us -> 0 us
  blocking collectives: 155 us -> 0 us
  Pallas kernels: 0 us -> 56.3 us
  matrix products: 24.2 us -> 0 us
  local copies, waits for them, and re-layouts: 3.39 us -> 20.5 us
  between operations: 14.6 us -> 0.64 us
  other arithmetic: 11.4 us -> 0 us
    psum x2 -> x0, waiting for transfers between devices: 173 us -> none  [finish(): total = lax.psum(partial_value, ('kv', 'tp'))]
    all_gather x5 -> x0, blocking collectives: 155 us -> none  [the longest x1 44 us: local(): lax.all_gather(tokens, ('kv', 'tp'), axis=1, tiled=True)]
    unnamed x6 -> x0, waiting for transfers between devices: 93.6 us -> none
    pallas_call x0 -> x1, Pallas kernels: none -> 56.3 us  [fused(): pl.pallas_call(functools.partial(layer_kernel, n_kv, n_tp), out_shape=(ja...]
    dot_general x10 -> x0, matrix products: 24.2 us -> none  [the longest x2 10.9 us: ffn_partial(): return jnp.dot(hidden, down_w, preferred_element_type=jnp.float32)]
    unnamed x22 -> x4, local copies, waits for them, and re-layouts: 3.12 us -> 20.5 us
    reduce_sum x7 -> x0, other arithmetic: 5.18 us -> none  [the longest x3 2.61 us: whole_norm(): spread = jnp.mean(centred * centred, axis=-1, keepdims=True)]
  transfers between devices with their start and end apart: 4 -> 0, of which waited for: 4 -> 0; matrix products, arithmetic and copies ran while one was open for 0% -> 0% of each run, Pallas kernels for 0% -> 0%
where the time goes in v1:
time: 78 us; the launch traced here: 77.5 us
  Pallas kernels  56.3 us (72%)
  local copies, waits for them, and re-layouts  20.5 us (26%)
    pallas_call x1, Pallas kernels, fused(): pl.pallas_call(functools.partial(layer_kernel, n_kv, n_tp), out_shape=(ja...  56.3 us
    unnamed x4, local copies, waits for them, and re-layouts  20.5 us

profile of v1, /device:TPU:0, one launch (start us, length us, event | category | flops | bytes accessed | tf_op | source)
XLA Modules:
  0.0 77.5 jit_solution(16923676231441206954)
XLA Ops:
  0.6 8.5 %copy.16.gate_hbm = bf16[2,4096,352]{2,1,0:T(8,128)(2,1)} copy(bf16[2,4096,352]{1,2,0:T(8,128)(2,1)} %param.15) | data formatting | bytes 11534336 | tf_op args[1]
  9.1 8.5 %copy.17.up_hbm = bf16[2,4096,352]{2,1,0:T(8,128)(2,1)} copy(bf16[2,4096,352]{1,2,0:T(8,128)(2,1)} %param.16) | data formatting | bytes 11534336 | tf_op args[2]
  17.6 56.3 %layer.1 = (bf16[16,128]{1,0:T(8,128)(2,1)}, f32[2,8,128,128]{3,2,1,0:T(8,128)}) custom-call(bf16[16,128]{1,0:T(8,128)(2,1)} %tokens_ref.1, bf16[3,128]{1,0:T(4,128)(2,1)} %gain_ref.1, bf16[3,128]{1,0:T(4,128)(2,1)} %bias_ref.1, f32[8,128]{1,0:T(8,128)} %bitcast.2, f32[8,128]{1,0:T(8,128)} %bitcast.3, bf16[2,4096,352]{2,1,0:T(8,128)(2,1)} %copy.16.gate_hbm, ...), custom_call_target="tpu_custom_call" | custom-call | tf_op jit(solution)/shard_map/layer/pallas_call | solution.py:521
  73.9 1.3 %copy.20 = bf16[16,128]{1,0:T(8,128)(2,1)} copy(bf16[16,128]{1,0:T(8,128)(2,1)} %get-tuple-element.4) | data formatting | bytes 8192
  75.2 2.3 %copy.21 = f32[2,8,128,128]{3,2,1,0:T(8,128)} copy(f32[2,8,128,128]{3,2,1,0:T(8,128)} %get-tuple-element.5) | data formatting | bytes 2097152

commit v2 on v1

--- a/solution.py
+++ b/solution.py
@@ -137,6 +137,12 @@
         rest = [terms[-1]] if len(terms) % 2 else []
         terms = [a + b for a, b in zip(terms[::2], terms[1::2])] + rest
     return terms[0]
+
+
+def dot_turned(rows, weights):
+    return lax.dot_general(
+        rows, weights, (((1,), (1,)), ((), ())), preferred_element_type=jnp.float32
+    )
 
 
 def layer_kernel(
@@ -272,16 +278,14 @@
 
     def ffn(rows, layer):
         step = 4 * lane
-        gate = jnp.zeros((batch, gate_v.shape[2]), jnp.float32)
-        up = jnp.zeros((batch, gate_v.shape[2]), jnp.float32)
+        gate = jnp.zeros((batch, gate_v.shape[1]), jnp.float32)
+        up = jnp.zeros((batch, gate_v.shape[1]), jnp.float32)
         loads["gate%d" % layer].wait()
         loads["up%d" % layer].wait()
         for k in range(0, width, step):
             piece = rows[:, k : k + step]
-            gate += jnp.dot(
-                piece, gate_v[layer, k : k + step, :], preferred_element_type=jnp.float32
-            )
-            up += jnp.dot(piece, up_v[layer, k : k + step, :], preferred_element_type=jnp.float32)
+            gate += dot_turned(piece, gate_v[layer, :, k : k + step])
+            up += dot_turned(piece, up_v[layer, :, k : k + step])
         hidden = (jax.nn.silu(gate) * up).astype(jnp.bfloat16)
         loads["down%d" % layer].wait()
         for k in range(0, width, step):
@@ -477,6 +481,8 @@
     batch, lane = tokens.shape
     n = n_kv * n_tp
     seqs, heads = state.shape[:2]
+    gate_weights = jnp.swapaxes(gate_weights, 1, 2)
+    up_weights = jnp.swapaxes(up_weights, 1, 2)
     bf16, f32 = jnp.bfloat16, jnp.float32
     per_seq = 4 * heads
     rows_tp = seqs * heads

time: 78 us -> 62.9 us (0.81)
  local copies, waits for them, and re-layouts: 20.5 us -> 3.57 us
  Pallas kernels: 56.3 us -> 58.5 us
    unnamed x4 -> x2, local copies, waits for them, and re-layouts: 20.5 us -> 3.57 us
    pallas_call x1, Pallas kernels: 56.3 us -> 58.5 us  [fused(): pl.pallas_call(functools.partial(layer_kernel, n_kv, n_tp), out_shape=(ja...]
where the time goes in v2:
time: 62.9 us; the launch traced here: 62.7 us
  Pallas kernels  58.5 us (93%)
  local copies, waits for them, and re-layouts  3.57 us (6%)
  between operations  0.64 us (1%)
    pallas_call x1, Pallas kernels, fused(): pl.pallas_call(functools.partial(layer_kernel, n_kv, n_tp), out_shape=(ja...  58.5 us
    unnamed x2, local copies, waits for them, and re-layouts  3.57 us

profile of v2, /device:TPU:0, one launch (start us, length us, event | category | flops | bytes accessed | tf_op | source)
XLA Modules:
  0.0 62.7 jit_solution(1397103277918815861)
XLA Ops:
  0.6 58.5 %layer.1 = (bf16[16,128]{1,0:T(8,128)(2,1)}, f32[2,8,128,128]{3,2,1,0:T(8,128)}) custom-call(bf16[16,128]{1,0:T(8,128)(2,1)} %tokens_ref.1, bf16[3,128]{1,0:T(4,128)(2,1)} %gain_ref.1, bf16[3,128]{1,0:T(4,128)(2,1)} %bias_ref.1, f32[8,128]{1,0:T(8,128)} %bitcast.6, f32[8,128]{1,0:T(8,128)} %bitcast.7, bf16[2,352,4096]{2,1,0:T(8,128)(2,1)} %bitcast.4, ...), custom_call_target="tpu_custom_call" | custom-call | tf_op jit(solution)/shard_map/layer/pallas_call | solution.py:527
  59.1 1.3 %copy.18 = bf16[16,128]{1,0:T(8,128)(2,1)} copy(bf16[16,128]{1,0:T(8,128)(2,1)} %get-tuple-element.4) | data formatting | bytes 8192
  60.4 2.3 %copy.19 = f32[2,8,128,128]{3,2,1,0:T(8,128)} copy(f32[2,8,128,128]{3,2,1,0:T(8,128)} %get-tuple-element.5) | data formatting | bytes 2097152

commit v3 on v2

--- a/solution.py
+++ b/solution.py
@@ -218,14 +218,18 @@
         loads[name] = pltpu.make_async_copy(source, target, load_sem.at[i])
         loads[name].start()
 
+    def turn(index, by, count):
+        moved = index + by
+        return jnp.where(moved >= count, moved - count, moved)
+
     def peer_id(k):
-        peer = lax.rem(me + k, n)
-        return peer, (lax.div(peer, n_tp), lax.rem(peer, n_tp))
+        far, near = divmod(k, n_tp)
+        peer = (turn(kv, far, n_kv), turn(tp, near, n_tp))
+        return peer[0] * n_tp + peer[1], peer
 
     barrier = pltpu.get_barrier_semaphore()
 
-    @pl.loop(1, n)
-    def _(k):
+    for k in range(1, n):
         _, device = peer_id(k)
         pl.semaphore_signal(barrier, inc=1, device_id=device, device_id_type=MESH)
 
@@ -233,8 +237,7 @@
         return ref.at[pl.ds(pl.multiple_of(index * rows, rows), rows)]
 
     def send_all(phase, src_of, dst, count, device_of):
-        @pl.loop(1, count)
-        def _(k):
+        for k in sorted(range(1, count), key=lambda k: abs(2 * k - count)):
             index, device = device_of(k)
             pltpu.make_async_remote_copy(
                 src_ref=src_of(index),
@@ -333,7 +336,7 @@
     block_len = seqs * per_seq
 
     def kv_peer(k):
-        peer = lax.rem(kv + k, n_kv)
+        peer = turn(kv, k, n_kv)
         return peer, (peer, tp)
 
     send_all(
@@ -398,7 +401,7 @@
     tp_send[...] = tp_f32[...].astype(jnp.bfloat16)
 
     def tp_peer(k):
-        peer = lax.rem(tp + k, n_tp)
+        peer = turn(tp, k, n_tp)
         return peer, (kv, peer)
 
     send_all(

time: 62.9 us -> 64 us (1.017)
  Pallas kernels: 58.5 us -> 59.6 us
    pallas_call x1, Pallas kernels: 58.5 us -> 59.6 us  [fused(): pl.pallas_call(functools.partial(layer_kernel, n_kv, n_tp), out_shape=(ja...]
where the time goes in v3:
time: 64 us; the launch traced here: 63.8 us
  Pallas kernels  59.6 us (93%)
  local copies, waits for them, and re-layouts  3.57 us (6%)
  between operations  0.64 us (1%)
    pallas_call x1, Pallas kernels, fused(): pl.pallas_call(functools.partial(layer_kernel, n_kv, n_tp), out_shape=(ja...  59.6 us
    unnamed x2, local copies, waits for them, and re-layouts  3.57 us

profile of v3, /device:TPU:0, one launch (start us, length us, event | category | flops | bytes accessed | tf_op | source)
XLA Modules:
  0.0 63.8 jit_solution(6330385108624117671)
XLA Ops:
  0.6 59.6 %layer.1 = (bf16[16,128]{1,0:T(8,128)(2,1)}, f32[2,8,128,128]{3,2,1,0:T(8,128)}) custom-call(bf16[16,128]{1,0:T(8,128)(2,1)} %tokens_ref.1, bf16[3,128]{1,0:T(4,128)(2,1)} %gain_ref.1, bf16[3,128]{1,0:T(4,128)(2,1)} %bias_ref.1, f32[8,128]{1,0:T(8,128)} %bitcast.6, f32[8,128]{1,0:T(8,128)} %bitcast.7, bf16[2,352,4096]{2,1,0:T(8,128)(2,1)} %bitcast.4, ...), custom_call_target="tpu_custom_call" | custom-call | tf_op jit(solution)/shard_map/layer/pallas_call | solution.py:530
  60.2 1.3 %copy.18 = bf16[16,128]{1,0:T(8,128)(2,1)} copy(bf16[16,128]{1,0:T(8,128)(2,1)} %get-tuple-element.4) | data formatting | bytes 8192
  61.5 2.3 %copy.19 = f32[2,8,128,128]{3,2,1,0:T(8,128)} copy(f32[2,8,128,128]{3,2,1,0:T(8,128)} %get-tuple-element.5) | data formatting | bytes 2097152
